TPU v7x, 256 devices: a 4x2x16 block of a 4x16x16 slice. The times are simulated.
256 devices in a mesh: grp: 2 (over y), sp: 32 (over z, core), tp: 4 (over x).
Axes of the slice: x: 4, y: 2, z: 16, core: 2. Of those that a mesh axis runs over, the one named last changes fastest.
The devices are a block of a 4x16x16 slice.
Arguments:
- conv_value: bfloat16 [32768, 1024], P(('grp', 'sp'), 'tp'), parts along dimension 0, may hold values from -6 to 6
- conv_gate: bfloat16 [32768, 1024], P(('grp', 'sp'), 'tp'), parts along dimension 0, may hold values from -6 to 6
- kernel: bfloat16 [31, 1024], P(None, 'tp'), may hold values from -4 to 4
- conv_bias: float32 [1024], P('tp'), may hold values from -3 to 3
- ln_gain: float32 [1024], P('tp'), may hold values from 0.1 to 1.9
- ln_bias: float32 [1024], P('tp'), may hold values from -3 to 3
- out_gain: float32 [1024], P('tp'), may hold values from 0.1 to 1.9
- out_weight: bfloat16 [1024, 2048], replicated, may hold values from -0.1875 to 0.1875
- residual: bfloat16 [32768, 2048], P(('grp', 'sp', 'tp')), parts along dimension 0, may hold values from -6 to 6
- moe_gain: float32 [2048], replicated, may hold values from 0.1 to 1.9
- expert_ids: int32 [32768, 2], P(('grp', 'sp', 'tp')), parts along dimension 0, may hold values from 0 to 127, as said below
- expert_weights: float32 [32768, 2], P(('grp', 'sp', 'tp')), parts along dimension 0, may hold values from 0.1 to 0.7
- w_gate: bfloat16 [128, 2048, 512], P(('sp', 'tp')), may hold values from -0.125 to 0.125
- w_up: bfloat16 [128, 2048, 512], P(('sp', 'tp')), may hold values from -0.125 to 0.125
- w_down: bfloat16 [128, 512, 2048], P(('sp', 'tp')), may hold values from -0.25 to 0.25
Outputs:
- layer_out: bfloat16 [32768, 2048], P(('grp', 'sp', 'tp')), parts along dimension 0
There are 2 independent parts, one for each index of `grp`. A program takes and returns all parts, laid end to end along the dimension named above; an argument that names none is the same for every part. Nothing has to cross between parts.
Inputs may be any that keep to these rules, and one draw needn't show every extreme that they name: `expert_ids`: each row names two different experts of one group (group = expert number // 32). Among the 128 rows of one device (aligned blocks of 128 rows) no expert is named more than 4 times, and in every such block some expert is named exactly 4 times.
All inputs are finite; a program needn't handle non-finite values.
Results may differ from a plain program's by a relative error of at most 0.0095.
Values may be sent and summed in bfloat16 or wider, within the bound.
A program may use at most 64 MiB of HBM per device.

v0:
```python
import jax
import jax.numpy as jnp
from jax import lax
from jax.sharding import PartitionSpec as P

EPSILON = 1e-06


def passed_along(block, axis, distance):
    devices = range(lax.axis_size(axis))
    route = [(i - distance, i) for i in devices if i - distance in devices]
    return lax.ppermute(block, axis, route)


def copy_for_each(shard, axis):
    size = lax.axis_size(axis)
    return lax.all_to_all(
        jnp.broadcast_to(shard[None], (size, *shard.shape)), axis, 0, 0, tiled=True
    )


def of_everyone(shard, axis):
    return copy_for_each(shard, axis).sum(axis=0)


def together(arrays, axis):
    ends = [0]
    for a in arrays:
        ends.append(ends[-1] + a.size)
    subtotal = of_everyone(jnp.concatenate([a.ravel() for a in arrays]), axis)
    return tuple((subtotal[b:e].reshape(a.shape) for a, b, e in zip(arrays, ends, ends[1:])))


def per_device(
    conv_value,
    conv_gate,
    kernel,
    conv_bias,
    ln_gain,
    ln_bias,
    out_gain,
    out_weight,
    residual,
    moe_gain,
    expert_ids,
    expert_weights,
    w_gate,
    w_up,
    w_down,
):
    tok_rows, channels = conv_value.shape
    reach_rows = kernel.shape[0] - 1
    full_channels = channels * lax.axis_size("tp")
    gated = (conv_value.astype(jnp.float32) * jax.nn.sigmoid(conv_gate.astype(jnp.float32))).astype(
        jnp.bfloat16
    )
    before = passed_along(gated[tok_rows - reach_rows :], "sp", 1)
    padded = jnp.concatenate([before, gated], axis=0)
    convolved = jnp.zeros((tok_rows, channels), jnp.float32) + conv_bias
    for offset in range(reach_rows + 1):
        convolved = convolved + padded[offset : offset + tok_rows].astype(jnp.float32) * kernel[
            offset
        ].astype(jnp.float32)
    totals = together((jnp.sum(convolved, axis=1), jnp.sum(convolved * convolved, axis=1)), "tp")
    average = (totals[0] / full_channels)[:, None]
    spread = (totals[1] / full_channels)[:, None] - average * average
    swished = jax.nn.silu((convolved - average) * lax.rsqrt(spread + EPSILON) * ln_gain + ln_bias)
    energy = of_everyone(jnp.sum(swished * swished, axis=1), "tp")
    branch = (swished * lax.rsqrt(energy / full_channels + EPSILON)[:, None] * out_gain).astype(
        jnp.bfloat16
    )
    row_count = tok_rows // lax.axis_size("tp")
    regrouped = lax.all_to_all(branch, "tp", split_axis=0, concat_axis=1, tiled=True)
    projected = jnp.dot(regrouped, out_weight, preferred_element_type=jnp.float32)
    hidden = (residual.astype(jnp.float32) + projected).astype(jnp.bfloat16)
    widened = hidden.astype(jnp.float32)
    normed = (
        widened * lax.rsqrt(jnp.mean(widened * widened, axis=1, keepdims=True) + EPSILON) * moe_gain
    ).astype(jnp.bfloat16)
    width = normed.shape[1]
    experts = lax.axis_size("sp") * lax.axis_size("tp")
    capacity = 2 * row_count // min(row_count, experts // 2)
    flat_ids = expert_ids.reshape(-1)
    onehot = (flat_ids[:, None] == jnp.arange(experts, dtype=jnp.int32)[None, :]).astype(jnp.int32)
    slot_rank = jnp.sum((jnp.cumsum(onehot, axis=0) - 1) * onehot, axis=1)
    position = flat_ids * capacity + slot_rank
    outgoing = (
        jnp.zeros((experts * capacity, width), jnp.bfloat16)
        .at[position]
        .set(jnp.repeat(normed, 2, axis=0))
    )
    outgoing = outgoing.reshape(experts, capacity, width)
    arriving = lax.all_to_all(outgoing, ("sp", "tp"), split_axis=0, concat_axis=0, tiled=True)
    flattened = arriving.reshape(-1, width)
    gate_part = jnp.dot(flattened, w_gate[0], preferred_element_type=jnp.float32)
    up_part = jnp.dot(flattened, w_up[0], preferred_element_type=jnp.float32)
    active = (jax.nn.silu(gate_part) * up_part).astype(jnp.bfloat16)
    result = jnp.dot(active, w_down[0], preferred_element_type=jnp.float32).astype(jnp.bfloat16)
    produced = result.reshape(arriving.shape)
    returned = lax.all_to_all(produced, ("sp", "tp"), split_axis=0, concat_axis=0, tiled=True)
    returned = returned.reshape(experts * capacity, width)
    picked = returned[position].reshape(row_count, 2, width)
    combined = jnp.sum(picked.astype(jnp.float32) * expert_weights[:, :, None], axis=1)
    return (widened + combined).astype(jnp.bfloat16)


def solution(mesh):
    in_specs = (
        P(("grp", "sp"), "tp"),
        P(("grp", "sp"), "tp"),
        P(None, "tp"),
        P("tp"),
        P("tp"),
        P("tp"),
        P("tp"),
        P(),
        P(("grp", "sp", "tp"), None),
        P(),
        P(("grp", "sp", "tp"), None),
        P(("grp", "sp", "tp"), None),
        P(("sp", "tp"), None, None),
        P(("sp", "tp"), None, None),
        P(("sp", "tp"), None, None),
    )
    out_specs = P(("grp", "sp", "tp"), None)
    return jax.shard_map(
        per_device, mesh=mesh, in_specs=in_specs, out_specs=out_specs, check_vma=False
    )
```

profile of v0, /device:TPU:33, one launch (start us, length us, event | category | flops | bytes accessed | tf_op | source)
XLA Modules:
  0.0 328.9 jit_solution(4955386901156573632)
XLA Ops:
  0.0 1.3 multiply_convert_fusion.2
  1.4 5.7 %collective-permute-start = (bf16[30,256]{1,0:T(8,128)(2,1)S(1)}, bf16[30,256]{1,0:T(8,128)(2,1)S(1)}, u32[]{:S(2)}, u32[]{:S(2)}) collective-permute-start(bf16[30,256]{1,0:T(8,128)(2,1)S(1)} %slice.266), channel_id=1, source_target_pairs={{0,4},{4,8},{8,12},{12,16},{16,20},{20,24},{24,28},{28,32},{32,36}... | collective-permute-start | bytes 46088 | tf_op jit(solution)/shard_map/ppermute | solution.py:12
  7.1 1.1 slice_convert_fusion.30
  8.2 0.8 copy.41
  9.0 0.1 eq.29
  9.1 0.1 copy.43
  9.2 0.2 fusion.47
  9.5 0.1 add_add_fusion
  9.6 1.0 slice_convert_fusion.29
  10.5 13.2 %collective-permute-done = bf16[30,256]{1,0:T(8,128)(2,1)S(1)} collective-permute-done((bf16[30,256]{1,0:T(8,128)(2,1)S(1)}, bf16[30,256]{1,0:T(8,128)(2,1)S(1)}, u32[]{:S(2)}, u32[]{:S(2)}) %collective-permute-start) | collective-permute-done | bytes 15392 | tf_op jit(solution)/shard_map/ppermute | solution.py:12
  23.8 3.2 fusion.52
  26.9 0.6 broadcast_in_dim.8
  27.5 3.3 %all-to-all-start = ((f32[4,1,1024]{2,1,0:T(1,128)}), f32[4,1,1024]{2,1,0:T(1,128)S(1)}, u32[]{:S(2)}, u32[]{:S(2)}) async-start(f32[4,1,1024]{2,1,0:T(1,128)} %broadcast_in_dim.8), calls=%async_computation | async-start | bytes 32768 | tf_op jit(solution)/shard_map/all_to_all | solution.py:17
  30.9 0.0 copy-done.2
  30.9 0.1 eq.25
  31.1 3.9 %all-to-all-done = f32[4,1,1024]{2,1,0:T(1,128)S(1)} async-done(((f32[4,1,1024]{2,1,0:T(1,128)}), f32[4,1,1024]{2,1,0:T(1,128)S(1)}, u32[]{:S(2)}, u32[]{:S(2)}) %all-to-all-start) | async-done | bytes 16416 | tf_op jit(solution)/shard_map/all_to_all | solution.py:17
  35.1 0.3 multiply_reduce_fusion.2
  35.4 0.6 broadcast_in_dim.9
  36.0 3.3 %all-to-all-start.1 = ((f32[4,1,512]{2,1,0:T(1,128)}), f32[4,1,512]{2,1,0:T(1,128)S(1)}, u32[]{:S(2)}, u32[]{:S(2)}) async-start(f32[4,1,512]{2,1,0:T(1,128)} %broadcast_in_dim.9), calls=%async_computation.1 | async-start | bytes 16384 | tf_op jit(solution)/shard_map/all_to_all | solution.py:17
  39.4 0.2 fusion.48
  39.6 0.1 copy.40
  39.7 0.1 mul.644
  39.8 3.6 %all-to-all-done.1 = f32[4,1,512]{2,1,0:T(1,128)S(1)} async-done(((f32[4,1,512]{2,1,0:T(1,128)}), f32[4,1,512]{2,1,0:T(1,128)S(1)}, u32[]{:S(2)}, u32[]{:S(2)}) %all-to-all-start.1) | async-done | bytes 8224 | tf_op jit(solution)/shard_map/all_to_all | solution.py:17
  43.5 0.0 copy-done.3
  43.5 0.8 multiply_convert_fusion.1
  44.3 3.5 %all-to-all-start.2 = ((bf16[4,128,256]{2,1,0:T(8,128)(2,1)}), bf16[4,128,256]{2,1,0:T(8,128)(2,1)S(1)}, u32[]{:S(2)}, u32[]{:S(2)}) async-start(bf16[4,128,256]{2,1,0:T(8,128)(2,1)} %bitcast.31), calls=%async_computation.2 | async-start | bytes 524288 | tf_op jit(solution)/shard_map/all_to_all | solution.py:73
  47.9 5.4 %all-to-all-done.2 = bf16[4,128,256]{2,1,0:T(8,128)(2,1)S(1)} async-done(((bf16[4,128,256]{2,1,0:T(8,128)(2,1)}), bf16[4,128,256]{2,1,0:T(8,128)(2,1)S(1)}, u32[]{:S(2)}, u32[]{:S(2)}) %all-to-all-start.2) | async-done | bytes 262176 | tf_op jit(solution)/shard_map/all_to_all | solution.py:73
  53.3 0.2 copy.39
  53.5 0.0 copy-start.1
  53.5 3.1 multiply_reduce_fusion.1
  56.6 0.2 multiply_convert_fusion
  56.8 1.6 broadcast_in_dim.11
  58.4 2.3 reshape.156
  60.7 4.4 %scatter_custom_fusion = bf16[512,2048]{1,0:T(8,128)(2,1)} fusion(s32[256]{0:T(256)S(1)} %bitcast.97, bf16[256,2048]{1,0:T(8,128)(2,1)} %reshape.156, bf16[]{:T(256)} %constant.15.clone.1), kind=kCustom, calls=%fused_computation.46 | custom fusion | bytes 2097664 | tf_op jit(solution)/shard_map/scatter | solution.py:90
  65.1 4.1 %reshape.108 = bf16[128,4,2048]{2,1,0:T(4,128)(2,1)} reshape(bf16[512,2048]{1,0:T(8,128)(2,1)} %scatter_custom_fusion) | data formatting | bytes 4194304 | tf_op jit(solution)/shard_map/reshape | solution.py:92
  69.2 114.7 %all_to_all.41 = bf16[128,4,2048]{2,1,0:T(4,128)(2,1)} all-to-all(bf16[128,4,2048]{2,1,0:T(4,128)(2,1)} %reshape.108), channel_id=1, replica_groups=mesh['grp'=2,'sp'=32,'tp'=4] {'sp','tp'}, dimensions={0} | all-to-all | bytes 4194304 | tf_op jit(solution)/shard_map/all_to_all | solution.py:93
  183.9 4.0 %reshape.109 = bf16[512,2048]{1,0:T(8,128)(2,1)} reshape(bf16[128,4,2048]{2,1,0:T(4,128)(2,1)} %all_to_all.41) | data formatting | bytes 4194304 | tf_op jit(solution)/shard_map/reshape | solution.py:94
  187.9 4.4 %fusion.5 = f32[512,512]{1,0:T(8,128)} fusion(bf16[512,2048]{1,0:T(8,128)(2,1)} %reshape.109, bf16[1,2048,512]{2,1,0:T(8,128)(2,1)} %param.27), kind=kOutput, calls=%fused_computation.38 | convolution fusion | flops 1073741824 | bytes 5242880 | tf_op jit(solution)/shard_map/dot_general | solution.py:95
  192.3 6.2 %convolution_convert_fusion = bf16[512,2048]{1,0:T(8,128)(2,1)} fusion(bf16[1,512,2048]{2,1,0:T(8,128)(2,1)S(1)} %copy-done, bf16[512,2048]{1,0:T(8,128)(2,1)} %reshape.109, bf16[1,2048,512]{2,1,0:T(8,128)(2,1)} %param.28, f32[512,512]{1,0:T(8,128)} %fusion.5), kind=kOutput, calls=%fused_computation.31 | convolution fusion | flops 2150105088 | bytes 9437184 | tf_op jit(solution)/shard_map/dot_general | solution.py:98
  198.5 4.1 %reshape.110 = bf16[128,4,2048]{2,1,0:T(4,128)(2,1)} reshape(bf16[512,2048]{1,0:T(8,128)(2,1)} %convolution_convert_fusion) | data formatting | bytes 4194304 | tf_op jit(solution)/shard_map/reshape | solution.py:99
  202.6 10.0 %all-to-all-start.4 = ((bf16[128,4,2048]{2,1,0:T(4,128)(2,1)}), bf16[128,4,2048]{2,1,0:T(4,128)(2,1)}, u32[]{:S(2)}, u32[]{:S(2)}) async-start(bf16[128,4,2048]{2,1,0:T(4,128)(2,1)} %reshape.110), calls=%async_computation.4 | async-start | bytes 4194304 | tf_op jit(solution)/shard_map/all_to_all | solution.py:100
  212.7 0.1 copy.45
  212.8 97.7 %all-to-all-done.4 = bf16[128,4,2048]{2,1,0:T(4,128)(2,1)} async-done(((bf16[128,4,2048]{2,1,0:T(4,128)(2,1)}), bf16[128,4,2048]{2,1,0:T(4,128)(2,1)}, u32[]{:S(2)}, u32[]{:S(2)}) %all-to-all-start.4) | async-done | bytes 2097184 | tf_op jit(solution)/shard_map/all_to_all | solution.py:100
  310.6 4.0 %reshape.111 = bf16[512,2048]{1,0:T(8,128)(2,1)} reshape(bf16[128,4,2048]{2,1,0:T(4,128)(2,1)} %all-to-all-done.4) | data formatting | bytes 4194304 | tf_op jit(solution)/shard_map/reshape | solution.py:101
  314.5 5.2 %gather_fusion = bf16[256,2048]{1,0:T(8,128)(2,1)} fusion(bf16[512,2048]{1,0:T(8,128)(2,1)} %reshape.111, s32[1024]{0:T(1024)S(1)} %pad_clamp_fusion), kind=kCustom, calls=%fused_computation | custom fusion | bytes 2098176 | tf_op jit(solution)/shard_map/gather | solution.py:102
  319.7 3.4 %reshape.143 = f32[128,2,2048]{2,1,0:T(2,128)} reshape(bf16[256,2048]{1,0:T(8,128)(2,1)} %gather_fusion) | data formatting | bytes 3145728 | tf_op jit(solution)/shard_map/convert_element_type | solution.py:103
  323.1 4.8 %multiply_reduce_fusion = f32[128,2048]{1,0:T(8,128)S(1)} fusion(f32[128,2,2048]{2,1,0:T(2,128)} %reshape.143, f32[128,2]{1,0:T(8,128)S(1)} %copy.45), kind=kLoop, calls=%fused_computation.40 | loop fusion | flops 786432 | bytes 3146752 | tf_op jit(solution)/shard_map/reduce_sum | solution.py:103
  327.9 0.9 add_convert_fusion
  (25 shorter events, 0.2 us)
Async XLA Ops:
  0.0 192.3 %copy-start = (bf16[1,512,2048]{2,1,0:T(8,128)(2,1)S(1)}, bf16[1,512,2048]{2,1,0:T(8,128)(2,1)}, u32[]{:S(2)}) copy-start(bf16[1,512,2048]{2,1,0:T(8,128)(2,1)} %param.29) | copy-start | bytes 6291460
  0.0 30.9 %copy-start.2 = (s32[128,2]{0,1:T(2,128)S(1)}, s32[128,2]{0,1:T(2,128)}, u32[]{:S(2)}) copy-start(s32[128,2]{0,1:T(2,128)} %param.25) | copy-start | bytes 3076
  0.0 35.1 %copy-start.6 = (f32[256]{0:T(256)S(1)}, f32[256]{0:T(256)}, u32[]{:S(2)}) copy-start(f32[256]{0:T(256)} %param.19) | copy-start | bytes 3076
  0.0 35.1 %copy-start.5 = (f32[256]{0:T(256)S(1)}, f32[256]{0:T(256)}, u32[]{:S(2)}) copy-start(f32[256]{0:T(256)} %param.20) | copy-start | bytes 3076
  0.0 43.5 %copy-start.3 = (f32[256]{0:T(256)S(1)}, f32[256]{0:T(256)}, u32[]{:S(2)}) copy-start(f32[256]{0:T(256)} %param.21) | copy-start | bytes 3076
  1.4 22.4 %collective-permute-start = (bf16[30,256]{1,0:T(8,128)(2,1)S(1)}, bf16[30,256]{1,0:T(8,128)(2,1)S(1)}, u32[]{:S(2)}, u32[]{:S(2)}) collective-permute-start(bf16[30,256]{1,0:T(8,128)(2,1)S(1)} %slice.266), channel_id=1, source_target_pairs={{0,4},{4,8},{8,12},{12,16},{16,20},{20,24},{24,28},{28,32},{32,36}... | collective-permute-start | bytes 46088 | tf_op jit(solution)/shard_map/ppermute | solution.py:12
  27.5 7.5 %all-to-all-start = ((f32[4,1,1024]{2,1,0:T(1,128)}), f32[4,1,1024]{2,1,0:T(1,128)S(1)}, u32[]{:S(2)}, u32[]{:S(2)}) async-start(f32[4,1,1024]{2,1,0:T(1,128)} %broadcast_in_dim.8), calls=%async_computation | async-start | bytes 32768 | tf_op jit(solution)/shard_map/all_to_all | solution.py:17
  36.0 7.4 %all-to-all-start.1 = ((f32[4,1,512]{2,1,0:T(1,128)}), f32[4,1,512]{2,1,0:T(1,128)S(1)}, u32[]{:S(2)}, u32[]{:S(2)}) async-start(f32[4,1,512]{2,1,0:T(1,128)} %broadcast_in_dim.9), calls=%async_computation.1 | async-start | bytes 16384 | tf_op jit(solution)/shard_map/all_to_all | solution.py:17
  44.3 8.9 %all-to-all-start.2 = ((bf16[4,128,256]{2,1,0:T(8,128)(2,1)}), bf16[4,128,256]{2,1,0:T(8,128)(2,1)S(1)}, u32[]{:S(2)}, u32[]{:S(2)}) async-start(bf16[4,128,256]{2,1,0:T(8,128)(2,1)} %bitcast.31), calls=%async_computation.2 | async-start | bytes 524288 | tf_op jit(solution)/shard_map/all_to_all | solution.py:73
  53.5 3.2 copy-start.1
  202.6 10.0 %copy-start.4 = (f32[128,2]{0,1:T(2,128)S(1)}, f32[128,2]{0,1:T(2,128)}, u32[]{:S(2)}) copy-start(f32[128,2]{0,1:T(2,128)} %param.26) | copy-start | bytes 3076
  202.6 107.9 %all-to-all-start.4 = ((bf16[128,4,2048]{2,1,0:T(4,128)(2,1)}), bf16[128,4,2048]{2,1,0:T(4,128)(2,1)}, u32[]{:S(2)}, u32[]{:S(2)}) async-start(bf16[128,4,2048]{2,1,0:T(4,128)(2,1)} %reshape.110), calls=%async_computation.4 | async-start | bytes 4194304 | tf_op jit(solution)/shard_map/all_to_all | solution.py:100
where the time goes:
time: 330 us; the launch traced here: 329 us
  waiting for transfers between devices  124 us (38%)
  blocking collectives  115 us (35%)
  local copies, waits for them, and re-layouts  36 us (11%)
  starting transfers between devices  26 us (8%)
  other arithmetic  14.2 us (4%)
  matrix products  13.8 us (4%)
    all_to_all x1, blocking collectives, per_device(): lax.all_to_all(outgoing, ('sp', 'tp'), split_axis=0, concat_axis=0, tiled...  115 us
    all_to_all x1, waiting for transfers between devices, per_device(): lax.all_to_all(produced, ('sp', 'tp'), split_axis=0, concat_axis=0, tiled...  97.7 us
    ppermute x1, waiting for transfers between devices, passed_along(): return lax.ppermute(block, axis, route)  13.2 us
    all_to_all x1, starting transfers between devices, per_device(): lax.all_to_all(produced, ('sp', 'tp'), split_axis=0, concat_axis=0, tiled...  10 us
    all_to_all x2, waiting for transfers between devices, copy_for_each(): lax.all_to_all(jnp.broadcast_to(shard[None], (size, *shard.shape)), axis,...  7.57 us
    all_to_all x2, starting transfers between devices, copy_for_each(): lax.all_to_all(jnp.broadcast_to(shard[None], (size, *shard.shape)), axis,...  6.69 us
  transfers between devices with their start and end apart: 5, of which 5 were waited for; matrix products, arithmetic and copies ran while one was open for 1% of the time, Pallas kernels for 0%

commit v1 on v0

--- a/solution.py
+++ b/solution.py
@@ -70,7 +70,16 @@
         jnp.bfloat16
     )
     row_count = tok_rows // lax.axis_size("tp")
-    regrouped = lax.all_to_all(branch, "tp", split_axis=0, concat_axis=1, tiled=True)
+    fit_the_run = lambda incoming_x, named_axis, dim_at, out_dim: jnp.concatenate(
+        jax.lax.all_to_all(
+            jnp.stack(jnp.split(incoming_x, jax.lax.axis_size(named_axis), axis=dim_at)),
+            axis_name=named_axis,
+            split_axis=0,
+            concat_axis=0,
+        ),
+        out_dim,
+    )
+    regrouped = fit_the_run(branch, "tp", 0, 1)
     projected = jnp.dot(regrouped, out_weight, preferred_element_type=jnp.float32)
     hidden = (residual.astype(jnp.float32) + projected).astype(jnp.bfloat16)
     widened = hidden.astype(jnp.float32)

time: 330 us -> 333 us (level)
  no operation moved by 1% of the time
where the time goes in v1:
time: 333 us; the launch traced here: 331 us
  waiting for transfers between devices  125 us (38%)
  blocking collectives  115 us (35%)
  local copies, waits for them, and re-layouts  38.3 us (12%)
  starting transfers between devices  26 us (8%)
  matrix products  13.8 us (4%)
  other arithmetic  13.3 us (4%)
    all_to_all x1, blocking collectives, per_device(): lax.all_to_all(outgoing, ('sp', 'tp'), split_axis=0, concat_axis=0, tiled...  115 us
    all_to_all x1, waiting for transfers between devices, per_device(): lax.all_to_all(produced, ('sp', 'tp'), split_axis=0, concat_axis=0, tiled...  97.7 us
    ppermute x1, waiting for transfers between devices, passed_along(): return lax.ppermute(block, axis, route)  14.2 us
    all_to_all x1, starting transfers between devices, per_device(): lax.all_to_all(produced, ('sp', 'tp'), split_axis=0, concat_axis=0, tiled...  10 us
    all_to_all x2, waiting for transfers between devices, copy_for_each(): lax.all_to_all(jnp.broadcast_to(shard[None], (size, *shard.shape)), axis,...  7.57 us
    all_to_all x2, starting transfers between devices, copy_for_each(): lax.all_to_all(jnp.broadcast_to(shard[None], (size, *shard.shape)), axis,...  6.69 us
  transfers between devices with their start and end apart: 5, of which 5 were waited for; matrix products, arithmetic and copies ran while one was open for 1% of the time, Pallas kernels for 0%

profile of v1, /device:TPU:33, one launch (start us, length us, event | category | flops | bytes accessed | tf_op | source)
XLA Modules:
  0.0 331.5 jit_solution(11082233588809008514)
XLA Ops:
  0.0 1.2 copy.33
  1.3 1.1 copy.34
  2.4 0.0 copy-start.5
  2.4 0.1 multiply_convert_fusion.2
  2.5 0.1 slice.266
  2.6 5.7 %collective-permute-start = (bf16[30,256]{0,1:T(8,128)(2,1)S(1)}, bf16[30,256]{0,1:T(8,128)(2,1)S(1)}, u32[]{:S(2)}, u32[]{:S(2)}) collective-permute-start(bf16[30,256]{0,1:T(8,128)(2,1)S(1)} %slice.266), channel_id=1, source_target_pairs={{0,4},{4,8},{8,12},{12,16},{16,20},{20,24},{24,28},{28,32},{32,36}... | collective-permute-start | bytes 46088 | tf_op jit(solution)/shard_map/ppermute | solution.py:12
  8.4 1.1 slice_convert_fusion.30
  9.5 0.8 copy.38
  10.2 0.1 eq.29
  10.4 0.1 copy.40
  10.5 0.2 fusion.47
  10.8 0.1 add_add_fusion
  10.9 14.2 %collective-permute-done = bf16[30,256]{0,1:T(8,128)(2,1)S(1)} collective-permute-done((bf16[30,256]{0,1:T(8,128)(2,1)S(1)}, bf16[30,256]{0,1:T(8,128)(2,1)S(1)}, u32[]{:S(2)}, u32[]{:S(2)}) %collective-permute-start) | collective-permute-done | bytes 15392 | tf_op jit(solution)/shard_map/ppermute | solution.py:12
  25.1 4.5 %fusion.52 = (f32[512]{0:T(512)S(1)}, f32[512]{0:T(512)S(1)}, f32[512,256]{0,1:T(8,128)S(1)}) fusion(f32[256]{0:T(256)S(1)} %bitcast.101, bf16[512,256]{0,1:T(8,128)(2,1)S(1)} %multiply_convert_fusion.2, f32[256]{0:T(256)S(1)} %bitcast.102, bf16[30,256]{0,1:T(8,128)(2,1)S(1)} %collective-permute-done, f32[256]{0:T(256)S(1)} %bitcast.73, ...), kind=kLoop, calls=%fused_computation.166 | loop fusion | flops 24378368 | bytes 838656 | tf_op jit(solution)/shard_map/reduce_sum | solution.py:64
  29.6 0.6 broadcast_in_dim.8
  30.2 3.3 %all-to-all-start = ((f32[4,1,1024]{2,1,0:T(1,128)}), f32[4,1,1024]{2,1,0:T(1,128)S(1)}, u32[]{:S(2)}, u32[]{:S(2)}) async-start(f32[4,1,1024]{2,1,0:T(1,128)} %broadcast_in_dim.8), calls=%async_computation | async-start | bytes 32768 | tf_op jit(solution)/shard_map/all_to_all | solution.py:17
  33.6 0.1 eq.25
  33.8 3.9 %all-to-all-done = f32[4,1,1024]{2,1,0:T(1,128)S(1)} async-done(((f32[4,1,1024]{2,1,0:T(1,128)}), f32[4,1,1024]{2,1,0:T(1,128)S(1)}, u32[]{:S(2)}, u32[]{:S(2)}) %all-to-all-start) | async-done | bytes 16416 | tf_op jit(solution)/shard_map/all_to_all | solution.py:17
  37.8 0.3 multiply_reduce_fusion.2
  38.0 0.6 broadcast_in_dim.9
  38.6 3.3 %all-to-all-start.1 = ((f32[4,1,512]{2,1,0:T(1,128)}), f32[4,1,512]{2,1,0:T(1,128)S(1)}, u32[]{:S(2)}, u32[]{:S(2)}) async-start(f32[4,1,512]{2,1,0:T(1,128)} %broadcast_in_dim.9), calls=%async_computation.1 | async-start | bytes 16384 | tf_op jit(solution)/shard_map/all_to_all | solution.py:17
  42.0 0.2 fusion.48
  42.2 0.1 copy.37
  42.3 0.1 mul.644
  42.4 3.6 %all-to-all-done.1 = f32[4,1,512]{2,1,0:T(1,128)S(1)} async-done(((f32[4,1,512]{2,1,0:T(1,128)}), f32[4,1,512]{2,1,0:T(1,128)S(1)}, u32[]{:S(2)}, u32[]{:S(2)}) %all-to-all-start.1) | async-done | bytes 8224 | tf_op jit(solution)/shard_map/all_to_all | solution.py:17
  46.1 0.1 multiply_convert_fusion.1
  46.3 0.7 pad_maximum_fusion.1
  47.0 3.5 %all-to-all-start.2 = ((bf16[4,128,256]{1,2,0:T(8,128)(2,1)}), bf16[4,128,256]{1,2,0:T(8,128)(2,1)S(1)}, u32[]{:S(2)}, u32[]{:S(2)}) async-start(bf16[4,128,256]{1,2,0:T(8,128)(2,1)} %pad_maximum_fusion.1), calls=%async_computation.2 | async-start | bytes 524288 | tf_op jit(solution)/shard_map/all_to_all | solution.py:74
  50.5 5.4 %all-to-all-done.2 = bf16[4,128,256]{1,2,0:T(8,128)(2,1)S(1)} async-done(((bf16[4,128,256]{1,2,0:T(8,128)(2,1)}), bf16[4,128,256]{1,2,0:T(8,128)(2,1)S(1)}, u32[]{:S(2)}, u32[]{:S(2)}) %all-to-all-start.2) | async-done | bytes 262176 | tf_op jit(solution)/shard_map/all_to_all | solution.py:74
  56.0 3.1 multiply_reduce_fusion.1
  59.1 0.2 multiply_convert_fusion
  59.3 1.6 broadcast_in_dim.11
  60.9 2.3 reshape.161
  63.2 4.4 %scatter_custom_fusion = bf16[512,2048]{1,0:T(8,128)(2,1)} fusion(s32[256]{0:T(256)S(1)} %bitcast.104, bf16[256,2048]{1,0:T(8,128)(2,1)} %reshape.161, bf16[]{:T(256)} %constant.15.clone.1), kind=kCustom, calls=%fused_computation.46 | custom fusion | bytes 2097664 | tf_op jit(solution)/shard_map/scatter | solution.py:99
  67.6 4.1 %reshape.113 = bf16[128,4,2048]{2,1,0:T(4,128)(2,1)} reshape(bf16[512,2048]{1,0:T(8,128)(2,1)} %scatter_custom_fusion) | data formatting | bytes 4194304 | tf_op jit(solution)/shard_map/reshape | solution.py:101
  71.7 114.8 %all_to_all.27 = bf16[128,4,2048]{2,1,0:T(4,128)(2,1)} all-to-all(bf16[128,4,2048]{2,1,0:T(4,128)(2,1)} %reshape.113), channel_id=1, replica_groups=mesh['grp'=2,'sp'=32,'tp'=4] {'sp','tp'}, dimensions={0} | all-to-all | bytes 4194304 | tf_op jit(solution)/shard_map/all_to_all | solution.py:102
  186.5 4.0 %reshape.114 = bf16[512,2048]{1,0:T(8,128)(2,1)} reshape(bf16[128,4,2048]{2,1,0:T(4,128)(2,1)} %all_to_all.27) | data formatting | bytes 4194304 | tf_op jit(solution)/shard_map/reshape | solution.py:103
  190.5 4.5 %fusion.5 = f32[512,512]{1,0:T(8,128)} fusion(bf16[512,2048]{1,0:T(8,128)(2,1)} %reshape.114, bf16[1,2048,512]{2,1,0:T(8,128)(2,1)} %param.27), kind=kOutput, calls=%fused_computation.38 | convolution fusion | flops 1073741824 | bytes 5242880 | tf_op jit(solution)/shard_map/dot_general | solution.py:104
  194.9 6.2 %convolution_convert_fusion = bf16[512,2048]{1,0:T(8,128)(2,1)} fusion(bf16[1,512,2048]{2,1,0:T(8,128)(2,1)S(1)} %copy-done, bf16[512,2048]{1,0:T(8,128)(2,1)} %reshape.114, bf16[1,2048,512]{2,1,0:T(8,128)(2,1)} %param.28, f32[512,512]{1,0:T(8,128)} %fusion.5), kind=kOutput, calls=%fused_computation.2 | convolution fusion | flops 2150105088 | bytes 9437184 | tf_op jit(solution)/shard_map/dot_general | solution.py:107
  201.1 4.1 %reshape.115 = bf16[128,4,2048]{2,1,0:T(4,128)(2,1)} reshape(bf16[512,2048]{1,0:T(8,128)(2,1)} %convolution_convert_fusion) | data formatting | bytes 4194304 | tf_op jit(solution)/shard_map/reshape | solution.py:108
  205.2 10.0 %all-to-all-start.4 = ((bf16[128,4,2048]{2,1,0:T(4,128)(2,1)}), bf16[128,4,2048]{2,1,0:T(4,128)(2,1)}, u32[]{:S(2)}, u32[]{:S(2)}) async-start(bf16[128,4,2048]{2,1,0:T(4,128)(2,1)} %reshape.115), calls=%async_computation.4 | async-start | bytes 4194304 | tf_op jit(solution)/shard_map/all_to_all | solution.py:109
  215.3 0.1 copy.42
  215.4 97.7 %all-to-all-done.4 = bf16[128,4,2048]{2,1,0:T(4,128)(2,1)} async-done(((bf16[128,4,2048]{2,1,0:T(4,128)(2,1)}), bf16[128,4,2048]{2,1,0:T(4,128)(2,1)}, u32[]{:S(2)}, u32[]{:S(2)}) %all-to-all-start.4) | async-done | bytes 2097184 | tf_op jit(solution)/shard_map/all_to_all | solution.py:109
  313.1 4.0 %reshape.116 = bf16[512,2048]{1,0:T(8,128)(2,1)} reshape(bf16[128,4,2048]{2,1,0:T(4,128)(2,1)} %all-to-all-done.4) | data formatting | bytes 4194304 | tf_op jit(solution)/shard_map/reshape | solution.py:110
  317.1 5.2 %gather_fusion = bf16[256,2048]{1,0:T(8,128)(2,1)} fusion(bf16[512,2048]{1,0:T(8,128)(2,1)} %reshape.116, s32[1024]{0:T(1024)S(1)} %pad_clamp_fusion), kind=kCustom, calls=%fused_computation | custom fusion | bytes 2098176 | tf_op jit(solution)/shard_map/gather | solution.py:111
  322.3 3.4 %reshape.148 = f32[128,2,2048]{2,1,0:T(2,128)} reshape(bf16[256,2048]{1,0:T(8,128)(2,1)} %gather_fusion) | data formatting | bytes 3145728 | tf_op jit(solution)/shard_map/convert_element_type | solution.py:112
  325.7 4.8 %multiply_reduce_fusion = f32[128,2048]{1,0:T(8,128)S(1)} fusion(f32[128,2,2048]{2,1,0:T(2,128)} %reshape.148, f32[128,2]{1,0:T(8,128)S(1)} %copy.42), kind=kLoop, calls=%fused_computation.40 | loop fusion | flops 786432 | bytes 3146752 | tf_op jit(solution)/shard_map/reduce_sum | solution.py:112
  330.5 0.9 add_convert_fusion
  (32 shorter events, 0.2 us)
Async XLA Ops:
  0.0 194.9 %copy-start = (bf16[1,512,2048]{2,1,0:T(8,128)(2,1)S(1)}, bf16[1,512,2048]{2,1,0:T(8,128)(2,1)}, u32[]{:S(2)}) copy-start(bf16[1,512,2048]{2,1,0:T(8,128)(2,1)} %param.29) | copy-start | bytes 6291460
  0.0 10.8 %copy-start.1 = (bf16[31,256]{1,0:T(8,128)(2,1)S(1)}, bf16[31,256]{1,0:T(8,128)(2,1)}, u32[]{:S(2)}) copy-start(bf16[31,256]{1,0:T(8,128)(2,1)} %param.17) | copy-start | bytes 47620
  0.0 33.6 %copy-start.3 = (s32[128,2]{0,1:T(2,128)S(1)}, s32[128,2]{0,1:T(2,128)}, u32[]{:S(2)}) copy-start(s32[128,2]{0,1:T(2,128)} %param.25) | copy-start | bytes 3076
  0.0 25.1 %copy-start.4 = (f32[256]{0:T(256)S(1)}, f32[256]{0:T(256)}, u32[]{:S(2)}) copy-start(f32[256]{0:T(256)} %param.18) | copy-start | bytes 3076
  0.0 37.7 %copy-start.8 = (f32[256]{0:T(256)S(1)}, f32[256]{0:T(256)}, u32[]{:S(2)}) copy-start(f32[256]{0:T(256)} %param.19) | copy-start | bytes 3076
  0.0 37.7 %copy-start.7 = (f32[256]{0:T(256)S(1)}, f32[256]{0:T(256)}, u32[]{:S(2)}) copy-start(f32[256]{0:T(256)} %param.20) | copy-start | bytes 3076
  2.4 43.7 %copy-start.5 = (f32[256]{0:T(256)S(1)}, f32[256]{0:T(256)}, u32[]{:S(2)}) copy-start(f32[256]{0:T(256)} %param.21) | copy-start | bytes 3076
  2.6 22.4 %collective-permute-start = (bf16[30,256]{0,1:T(8,128)(2,1)S(1)}, bf16[30,256]{0,1:T(8,128)(2,1)S(1)}, u32[]{:S(2)}, u32[]{:S(2)}) collective-permute-start(bf16[30,256]{0,1:T(8,128)(2,1)S(1)} %slice.266), channel_id=1, source_target_pairs={{0,4},{4,8},{8,12},{12,16},{16,20},{20,24},{24,28},{28,32},{32,36}... | collective-permute-start | bytes 46088 | tf_op jit(solution)/shard_map/ppermute | solution.py:12
  30.2 7.5 %all-to-all-start = ((f32[4,1,1024]{2,1,0:T(1,128)}), f32[4,1,1024]{2,1,0:T(1,128)S(1)}, u32[]{:S(2)}, u32[]{:S(2)}) async-start(f32[4,1,1024]{2,1,0:T(1,128)} %broadcast_in_dim.8), calls=%async_computation | async-start | bytes 32768 | tf_op jit(solution)/shard_map/all_to_all | solution.py:17
  38.6 7.4 %all-to-all-start.1 = ((f32[4,1,512]{2,1,0:T(1,128)}), f32[4,1,512]{2,1,0:T(1,128)S(1)}, u32[]{:S(2)}, u32[]{:S(2)}) async-start(f32[4,1,512]{2,1,0:T(1,128)} %broadcast_in_dim.9), calls=%async_computation.1 | async-start | bytes 16384 | tf_op jit(solution)/shard_map/all_to_all | solution.py:17
  47.0 8.9 %all-to-all-start.2 = ((bf16[4,128,256]{1,2,0:T(8,128)(2,1)}), bf16[4,128,256]{1,2,0:T(8,128)(2,1)S(1)}, u32[]{:S(2)}, u32[]{:S(2)}) async-start(bf16[4,128,256]{1,2,0:T(8,128)(2,1)} %pad_maximum_fusion.1), calls=%async_computation.2 | async-start | bytes 524288 | tf_op jit(solution)/shard_map/all_to_all | solution.py:74
  56.0 3.1 copy-start.2
  205.2 10.0 %copy-start.6 = (f32[128,2]{0,1:T(2,128)S(1)}, f32[128,2]{0,1:T(2,128)}, u32[]{:S(2)}) copy-start(f32[128,2]{0,1:T(2,128)} %param.26) | copy-start | bytes 3076
  205.2 107.9 %all-to-all-start.4 = ((bf16[128,4,2048]{2,1,0:T(4,128)(2,1)}), bf16[128,4,2048]{2,1,0:T(4,128)(2,1)}, u32[]{:S(2)}, u32[]{:S(2)}) async-start(bf16[128,4,2048]{2,1,0:T(4,128)(2,1)} %reshape.115), calls=%async_computation.4 | async-start | bytes 4194304 | tf_op jit(solution)/shard_map/all_to_all | solution.py:109
